TPU v7x, 32 devices: a whole 2x2x4 slice. The times are simulated.
32 devices in a mesh: ep: 4 (over z), tp: 8 (over y, x, core).
Axes of the slice: x: 2, y: 2, z: 4, core: 2. Of those that a mesh axis runs over, the one named last changes fastest.
Arguments:
- hidden_in: bfloat16 [48, 2048], P('ep', 'tp'), may hold values from -12 to 12
- state: float32 [48, 32, 128, 128], P('ep', 'tp'), may hold values from -3 to 3
- lower_bound: float32 [32, 128], P('tp'), may hold values from 0.05 to 0.95
- w_forget: bfloat16 [2048, 4096], P(None, 'tp'), may hold values from -0.125 to 0.125
- w_input: bfloat16 [2048, 4096], P(None, 'tp'), may hold values from -0.125 to 0.125
- w_query: bfloat16 [2048, 4096], P(None, 'tp'), may hold values from -0.125 to 0.125
- w_outgate: bfloat16 [2048, 4096], P(None, 'tp'), may hold values from -0.125 to 0.125
- head_gain: float32 [128], replicated, may hold values from 0.1 to 1.9
- w_out: bfloat16 [4096, 2048], P('tp'), may hold values from -0.125 to 0.125
- ln1_gain: float32 [2048], replicated, may hold values from 0.1 to 8
- ln1_bias: float32 [2048], replicated, may hold values from -1.5 to 1.5
- routes: int32 [48, 4], P('ep'), may hold values from 0 to 7, all different within a row; in each aligned block of 12 rows (0 to 11, 12 to 23, ...) at most 9 rows name the same one
- route_weights: float32 [48, 4], P('ep'), may hold values from 0.2 to 1.5
- exp_gate: bfloat16 [8, 2048, 4096], P('ep', None, 'tp'), may hold values from -0.125 to 0.125
- exp_up: bfloat16 [8, 2048, 4096], P('ep', None, 'tp'), may hold values from -0.125 to 0.125
- exp_down: bfloat16 [8, 4096, 2048], P('ep', 'tp'), may hold values from -0.125 to 0.125
- sh_gate: bfloat16 [2048, 512], P(None, 'tp'), may hold values from -0.125 to 0.125
- sh_up: bfloat16 [2048, 512], P(None, 'tp'), may hold values from -0.125 to 0.125
- sh_down: bfloat16 [512, 2048], P('tp'), may hold values from -0.25 to 0.25
- ln2_gain: float32 [2048], replicated, may hold values from 0.1 to 1.9
- ln2_bias: float32 [2048], replicated, may hold values from -1.5 to 1.5
Outputs:
- mixed_out: bfloat16 [48, 2048], P('ep', 'tp')
- new_state: float32 [48, 32, 128, 128], P('ep', 'tp')
Inputs may be any that keep to these rules, and one draw needn't show every extreme that they name: `routes`: each row names 4 different experts; among the rows of one index of ep (12 rows) no expert is named more than 9 times, a bound that some block reaches.
All inputs are finite; a program needn't handle non-finite values.
Results may differ from a plain program's by a relative error of at most 0.023.
Values may be sent and summed in bfloat16 or wider, within the bound.
A program may use at most 64 MiB of HBM per device.

v0:
```python
import jax
import jax.numpy as jnp
from jax import lax
from jax.sharding import PartitionSpec as P

EPS = 1e-05
ALPHA = 2.0**0.25


def rounded(value):
    return lax.optimization_barrier(value.astype(jnp.bfloat16)).astype(jnp.float32)


def local(
    hidden_in,
    state,
    lower_bound,
    w_forget,
    w_input,
    w_query,
    w_outgate,
    head_gain,
    w_out,
    ln1_gain,
    ln1_bias,
    routes,
    route_weights,
    exp_gate,
    exp_up,
    exp_down,
    sh_gate,
    sh_up,
    sh_down,
    ln2_gain,
    ln2_bias,
):
    n_tp = lax.axis_size("tp")
    n_ep = lax.axis_size("ep")
    seq_count = hidden_in.shape[0]
    col_count = hidden_in.shape[1]
    model_width = col_count * n_tp
    col_start = lax.axis_index("tp") * col_count
    heads_dev = state.shape[1]
    head_size = state.shape[2]
    top_count = routes.shape[1]
    local_experts = exp_gate.shape[0]
    expert_count = local_experts * n_ep
    capacity = max(2, 3 * seq_count * top_count // (2 * expert_count))
    slot_count = expert_count * capacity
    rows_full = lax.all_gather(hidden_in, "tp", axis=1, tiled=True)

    def project(weight):
        product = jnp.dot(rows_full, weight, preferred_element_type=jnp.float32)
        return rounded(product).reshape(seq_count, heads_dev, head_size)

    forget_pre = project(w_forget)
    forget = lower_bound + (1.0 - lower_bound) * jax.nn.sigmoid(forget_pre)
    key_part = (1.0 - lower_bound) * jax.nn.sigmoid(-forget_pre)
    values = project(w_input)
    queries = jax.nn.silu(project(w_query))
    out_gate = jax.nn.silu(project(w_outgate))
    new_state = forget[..., None] * state + key_part[..., None] * values[:, :, None, :]
    readout = jnp.einsum("bhd,bhdv->bhv", queries, new_state, precision=lax.Precision.HIGHEST)
    normed = readout * lax.rsqrt(jnp.mean(readout * readout, -1, keepdims=True) + EPS) * head_gain
    mixed = (normed * out_gate).astype(jnp.bfloat16).reshape(seq_count, heads_dev * head_size)
    branch = jnp.dot(mixed, w_out, preferred_element_type=jnp.float32)
    summed = lax.psum(branch.astype(jnp.bfloat16), "tp").astype(jnp.float32)
    residual = ALPHA * rows_full.astype(jnp.float32) + summed
    average = jnp.mean(residual, -1, keepdims=True)
    centered = residual - average
    variance = jnp.mean(centered * centered, -1, keepdims=True)
    normed_rows = (centered * lax.rsqrt(variance + EPS) * ln1_gain + ln1_bias).astype(jnp.bfloat16)
    routes_flat = routes.reshape(-1)
    one_hot = (routes_flat[:, None] == jnp.arange(expert_count, dtype=jnp.int32)[None, :]).astype(
        jnp.int32
    )
    position = jnp.sum((jnp.cumsum(one_hot, 0) - one_hot) * one_hot, 1)
    slot_index = routes_flat * capacity + position
    placing = (slot_index[:, None] == jnp.arange(slot_count, dtype=jnp.int32)[None, :]).astype(
        jnp.float32
    )
    chooser = jnp.sum(placing.reshape(seq_count, top_count, slot_count), 1).astype(jnp.bfloat16)
    weighted = jnp.sum(
        (placing * route_weights.reshape(-1)[:, None]).reshape(seq_count, top_count, slot_count), 1
    )
    own_cols = lax.dynamic_slice_in_dim(normed_rows, col_start, col_count, 1)
    picked = lax.dot_general(
        chooser, normed_rows, (((0,), (0,)), ((), ())), preferred_element_type=jnp.float32
    )
    arrived = lax.all_to_all(
        picked.astype(jnp.bfloat16).reshape(n_ep, local_experts * capacity, normed_rows.shape[1]),
        "ep",
        split_axis=0,
        concat_axis=0,
        tiled=True,
    )
    blocks = arrived.reshape(n_ep, local_experts, capacity, model_width)
    gate_part = jnp.einsum("gecd,edf->gecf", blocks, exp_gate, preferred_element_type=jnp.float32)
    up_part = jnp.einsum("gecd,edf->gecf", blocks, exp_up, preferred_element_type=jnp.float32)
    hidden_part = (jax.nn.silu(gate_part) * up_part).astype(jnp.bfloat16)
    expert_part = jnp.einsum(
        "gecf,efd->gecd", hidden_part, exp_down, preferred_element_type=jnp.float32
    )
    expert_part = expert_part.reshape(n_ep, local_experts * capacity, model_width).astype(
        jnp.bfloat16
    )
    shared_hidden = (
        jax.nn.silu(jnp.dot(normed_rows, sh_gate, preferred_element_type=jnp.float32))
        * jnp.dot(normed_rows, sh_up, preferred_element_type=jnp.float32)
    ).astype(jnp.bfloat16)
    shared_part = jnp.dot(shared_hidden, sh_down, preferred_element_type=jnp.float32)
    returned = lax.all_to_all(expert_part, "ep", split_axis=0, concat_axis=0, tiled=True)
    routed_partial = jnp.dot(
        weighted,
        returned.reshape(slot_count, model_width).astype(jnp.float32),
        precision=lax.Precision.HIGHEST,
    )
    combined = lax.psum_scatter(
        (routed_partial + shared_part).astype(jnp.bfloat16), "tp", scatter_dimension=1, tiled=True
    ).astype(jnp.float32)
    final_in = ALPHA * own_cols.astype(jnp.float32) + combined
    moments_two = lax.psum((jnp.sum(final_in, -1), jnp.sum(final_in * final_in, -1)), "tp")
    average_two = moments_two[0][:, None] / model_width
    variance_two = moments_two[1][:, None] / model_width - average_two * average_two
    gain_two = lax.dynamic_slice_in_dim(ln2_gain, col_start, col_count)
    bias_two = lax.dynamic_slice_in_dim(ln2_bias, col_start, col_count)
    mixed_out = (
        (final_in - average_two) * lax.rsqrt(variance_two + EPS) * gain_two + bias_two
    ).astype(jnp.bfloat16)
    return (mixed_out, new_state)


def solution(mesh):
    placed = (
        P("ep", "tp"),
        P("ep", "tp", None, None),
        P("tp", None),
        P(None, "tp"),
        P(None, "tp"),
        P(None, "tp"),
        P(None, "tp"),
        P(),
        P("tp", None),
        P(),
        P(),
        P("ep", None),
        P("ep", None),
        P("ep", None, "tp"),
        P("ep", None, "tp"),
        P("ep", "tp", None),
        P(None, "tp"),
        P(None, "tp"),
        P("tp", None),
        P(),
        P(),
    )
    return jax.shard_map(
        local,
        mesh=mesh,
        in_specs=placed,
        out_specs=(P("ep", "tp"), P("ep", "tp", None, None)),
        check_vma=False,
    )
```

profile of v0, /device:TPU:0, one launch (start us, length us, event | category | flops | bytes accessed | tf_op | source)
XLA Modules:
  0.0 155.0 jit_solution(1456552702936218920)
XLA Ops:
  7.2 0.0 copy-start
  7.2 0.9 copy.41
  8.1 0.1 eq.30
  8.2 0.1 fusion.39
  8.3 0.1 reduce_window_sum.11
  8.3 0.2 select_reduce_fusion.1
  8.5 0.1 reduce_sum.78
  8.6 0.8 copy.43
  9.4 10.7 %all_gather.3 = bf16[12,2048]{1,0:T(8,128)(2,1)S(1)} all-gather(bf16[12,256]{1,0:T(8,128)(2,1)} %param.21), channel_id=1, replica_groups=mesh['ep'=4,'tp'=8] {'tp'}, dimensions={1}, use_global_device_ids=true | all-gather | bytes 55296 | tf_op jit(solution)/shard_map/all_gather | solution.py:50
  20.1 2.0 %convolution_convert_fusion.2 = bf16[12,512]{1,0:T(8,128)(2,1)S(1)} fusion(bf16[12,2048]{1,0:T(8,128)(2,1)S(1)} %all_gather.3, bf16[2048,512]{1,0:T(8,128)(2,1)} %param.27), kind=kOutput, calls=%fused_computation.17 | convolution fusion | flops 25171968 | bytes 2158592 | tf_op jit(solution)/shard_map/dot_general | solution.py:53
  22.1 0.0 copy-start.3
  22.1 2.0 %convolution_convert_fusion.5 = bf16[12,512]{1,0:T(8,128)(2,1)S(1)} fusion(bf16[12,2048]{1,0:T(8,128)(2,1)S(1)} %all_gather.3, bf16[2048,512]{1,0:T(8,128)(2,1)} %param.26), kind=kOutput, calls=%fused_computation.20 | convolution fusion | flops 25171968 | bytes 2158592 | tf_op jit(solution)/shard_map/dot_general | solution.py:53
  24.1 2.0 %convolution_convert_fusion.3 = bf16[12,512]{1,0:T(8,128)(2,1)S(1)} fusion(bf16[12,2048]{1,0:T(8,128)(2,1)S(1)} %all_gather.3, bf16[2048,512]{1,0:T(8,128)(2,1)} %param.25), kind=kOutput, calls=%fused_computation.18 | convolution fusion | flops 25171968 | bytes 2158592 | tf_op jit(solution)/shard_map/dot_general | solution.py:53
  26.1 2.0 %convolution_convert_fusion.4 = bf16[12,512]{1,0:T(8,128)(2,1)S(1)} fusion(bf16[12,2048]{1,0:T(8,128)(2,1)S(1)} %all_gather.3, bf16[2048,512]{1,0:T(8,128)(2,1)} %param.24), kind=kOutput, calls=%fused_computation.19 | convolution fusion | flops 25171968 | bytes 2158592 | tf_op jit(solution)/shard_map/dot_general | solution.py:53
  28.3 3.8 %multiply_add_fusion = f32[12,4,128,128]{3,2,1,0:T(8,128)S(1)} fusion(f32[12,4,128,128]{3,2,1,0:T(8,128)} %param.22, f32[12,4,128]{2,1,0:T(4,128)S(1)} %reshape.140, f32[12,4,128]{2,1,0:T(4,128)S(1)} %bitcast.85, f32[12,4,128]{2,1,0:T(4,128)S(1)} %bitcast.84), kind=kLoop, calls=%fused_computation.6 | loop fusion | flops 2359296 | bytes 6365184 | tf_op jit(solution)/shard_map/add | solution.py:62
  32.1 0.0 copy-start.1
  32.1 1.6 %copy-done.1 = f32[12,4,128,128]{3,2,1,0:T(8,128)} copy-done((f32[12,4,128,128]{3,2,1,0:T(8,128)}, f32[12,4,128,128]{3,2,1,0:T(8,128)S(1)}, u32[]{:S(2)}) %copy-start.1) | copy-done | bytes 3145752
  33.7 2.8 %fusion.51 = f32[12,4,1,128]{3,2,1,0:T(1,128)S(1)} fusion(f32[12,4,128,1]{2,3,1,0:T(1,128)S(1)} %bitcast.83, f32[12,4,128,128]{3,2,1,0:T(8,128)S(1)} %multiply_add_fusion), kind=kOutput, calls=%fused_computation.69 | convolution fusion | flops 9437184 | bytes 3194880 | tf_op jit(solution)/shard_map/bhd,bhdv->bhv/dot_general | solution.py:63
  36.5 0.1 multiply_reduce_fusion.1
  36.6 0.1 fusion.40
  36.7 0.4 convolution_convert_fusion.1
  37.1 23.9 %psum.21 = bf16[12,2048]{1,0:T(8,128)(2,1)S(1)} all-reduce(bf16[12,2048]{1,0:T(8,128)(2,1)S(1)} %convolution_convert_fusion.1), channel_id=1, replica_groups=mesh['ep'=4,'tp'=8] {'tp'}, use_global_device_ids=true, to_apply=%region_1.2 | all-reduce | flops 24576 | bytes 98304 | tf_op jit(solution)/shard_map/psum | solution.py:67
  61.0 0.1 fusion.28
  61.1 0.2 multiply_reduce_fusion
  61.4 0.1 convert_reduce_fusion
  61.5 0.1 add_convert_fusion
  61.6 0.3 convolution_convert_fusion
  61.9 0.1 reshape.135
  62.0 13.9 %all_to_all.10 = bf16[4,18,2048]{2,1,0:T(8,128)(2,1)S(1)} all-to-all(bf16[4,18,2048]{2,1,0:T(8,128)(2,1)S(1)} %reshape.135), channel_id=1, replica_groups=mesh['ep'=4,'tp'=8] {'ep'}, dimensions={0} | all-to-all | bytes 589824 | tf_op jit(solution)/shard_map/all_to_all | solution.py:90
  75.8 0.2 copy.44
  76.0 2.9 %fusion.13 = f32[4,2,9,512]{3,2,0,1:T(8,128)S(1)} fusion(bf16[2,2048,512]{2,1,0:T(8,128)(2,1)} %param.34, bf16[4,2,9,2048]{3,0,2,1:T(4,128)(2,1)S(1)} %bitcast.78), kind=kOutput, calls=%fused_computation.13 | convolution fusion | flops 150994944 | bytes 4636672 | tf_op jit(solution)/shard_map/gecd,edf->gecf/dot_general | solution.py:98
  79.0 5.0 %fusion.9 = bf16[4,2,9,2048]{3,2,0,1:T(8,128)(2,1)S(1)} fusion(bf16[2,512,2048]{2,1,0:T(8,128)(2,1)} %param.36, bf16[2,2048,512]{2,1,0:T(8,128)(2,1)} %param.35, bf16[4,2,9,2048]{3,0,2,1:T(4,128)(2,1)S(1)} %bitcast.79, f32[4,2,9,512]{3,2,0,1:T(8,128)S(1)} %fusion.13), kind=kOutput, calls=%fused_computation.8 | convolution fusion | flops 302358528 | bytes 9125888 | tf_op jit(solution)/shard_map/gecf,efd->gecd/dot_general | solution.py:101
  84.0 0.2 copy.47
  84.2 0.9 copy.48
  85.2 3.5 %all-to-all-start.1 = ((bf16[4,18,2048]{2,1,0:T(8,128)(2,1)}), bf16[4,18,2048]{2,1,0:T(8,128)(2,1)S(1)}, u32[]{:S(2)}, u32[]{:S(2)}) async-start(bf16[4,18,2048]{2,1,0:T(8,128)(2,1)} %copy.48), calls=%async_computation.1 | async-start | bytes 786432 | tf_op jit(solution)/shard_map/all_to_all | solution.py:112
  88.6 0.0 reduce-scatter.2.cloned.1.call-start
  88.7 1.1 fusion.53
  89.8 8.4 %all-to-all-done.1 = bf16[4,18,2048]{2,1,0:T(8,128)(2,1)S(1)} async-done(((bf16[4,18,2048]{2,1,0:T(8,128)(2,1)}), bf16[4,18,2048]{2,1,0:T(8,128)(2,1)S(1)}, u32[]{:S(2)}, u32[]{:S(2)}) %all-to-all-start.1) | async-done | bytes 294944 | tf_op jit(solution)/shard_map/all_to_all | solution.py:112
  98.2 0.1 reshape.137
  98.2 0.3 fusion.52
  98.5 2.0 %fusion.12 = bf16[12,2048]{1,0:T(8,128)(2,1)} fusion(f32[12,2048]{1,0:T(8,128)S(1)} %fusion.52, bf16[64,2048]{1,0:T(8,128)(2,1)S(1)} %copy-done.2, bf16[12,2048]{1,0:T(8,128)(2,1)S(1)} %add_convert_fusion, bf16[2048,64]{0,1:T(8,128)(2,1)} %param.38, f32[12,64]{1,0:T(8,128)S(1)} %fusion.53), kind=kOutput, calls=%fused_computation.11 | convolution fusion | flops 6345216 | bytes 723968 | tf_op jit(solution)/shard_map/dot_general | solution.py:111
  100.5 0.0 reduce-scatter.2.cloned.1.call-update
  100.5 0.8 dynamic_slice.11
  101.3 0.8 dynamic_slice.10
  102.0 31.7 %reduce-scatter.2.cloned.1.call-done = bf16[12,256]{1,0:T(8,128)(2,1)} async-done(((bf16[12,2048]{1,0:T(8,128)(2,1)}), bf16[12,256]{1,0:T(8,128)(2,1)}) %reduce-scatter.2.cloned.1.call-update) | async-done | bytes 6160 | tf_op jit(solution)/shard_map/reduce_scatter | solution.py:118
  133.8 0.8 fusion.41
  134.6 12.2 %all-reduce = (f32[12]{0:T(128)S(1)}, f32[12]{0:T(128)S(1)}) all-reduce(f32[12]{0:T(128)S(1)} %get-tuple-element.3, f32[12]{0:T(128)S(1)} %get-tuple-element.2), channel_id=1, replica_groups=mesh['ep'=4,'tp'=8] {'tp'}, use_global_device_ids=true, to_apply=%region_12.13 | all-reduce | flops 24 | bytes 192 | tf_op jit(solution)/shard_map/psum | solution.py:122
  146.8 1.4 add_convert_fusion.1
  (28 shorter events, 0.3 us)
Async XLA Ops:
  7.2 29.6 %copy-start = (bf16[512,2048]{1,0:T(8,128)(2,1)S(1)}, bf16[512,2048]{1,0:T(8,128)(2,1)}, u32[]{:S(2)}) copy-start(bf16[512,2048]{1,0:T(8,128)(2,1)} %param.29) | copy-start | bytes 6291460
  22.1 6.1 %copy-start.3 = (f32[4,128]{1,0:T(4,128)S(1)}, f32[4,128]{1,0:T(4,128)}, u32[]{:S(2)}) copy-start(f32[4,128]{1,0:T(4,128)} %param.23) | copy-start | bytes 6148
  32.1 1.7 %copy-start.1 = (f32[12,4,128,128]{3,2,1,0:T(8,128)}, f32[12,4,128,128]{3,2,1,0:T(8,128)S(1)}, u32[]{:S(2)}) copy-start(f32[12,4,128,128]{3,2,1,0:T(8,128)S(1)} %multiply_add_fusion) | copy-start | bytes 9437188
  32.1 4.5 %copy-start.6 = (f32[128]{0:T(128)S(1)}, f32[128]{0:T(128)}, u32[]{:S(2)}) copy-start(f32[128]{0:T(128)} %param.28) | copy-start | bytes 1540
  32.1 29.4 %copy-start.4 = (f32[2048]{0:T(1024)S(1)}, f32[2048]{0:T(1024)}, u32[]{:S(2)}) copy-start(f32[2048]{0:T(1024)} %param.31) | copy-start | bytes 24580
  32.1 29.4 %copy-start.5 = (f32[2048]{0:T(1024)S(1)}, f32[2048]{0:T(1024)}, u32[]{:S(2)}) copy-start(f32[2048]{0:T(1024)} %param.30) | copy-start | bytes 24580
  84.0 14.5 %copy-start.2 = (bf16[64,2048]{1,0:T(8,128)(2,1)S(1)}, bf16[64,2048]{1,0:T(8,128)(2,1)}, u32[]{:S(2)}) copy-start(bf16[64,2048]{1,0:T(8,128)(2,1)} %param.39) | copy-start | bytes 786436
  85.2 13.0 %all-to-all-start.1 = ((bf16[4,18,2048]{2,1,0:T(8,128)(2,1)}), bf16[4,18,2048]{2,1,0:T(8,128)(2,1)S(1)}, u32[]{:S(2)}, u32[]{:S(2)}) async-start(bf16[4,18,2048]{2,1,0:T(8,128)(2,1)} %copy.48), calls=%async_computation.1 | async-start | bytes 786432 | tf_op jit(solution)/shard_map/all_to_all | solution.py:112
  88.6 45.2 %reduce-scatter.2.cloned.1.call-start = ((), (), s32[]{:S(2)}) async-start(), calls=%async_computation.3 | async-start | bytes 73728 | tf_op jit(solution)/shard_map/reduce_scatter | solution.py:118
Sparse Core Ops, SparseCore 0:
  100.6 33.1 reduce-scatter.1
where the time goes:
time: 156 us; the launch traced here: 155 us
  blocking collectives  60.6 us (39%)
  waiting for transfers between devices  40.1 us (26%)
  matrix products  22.5 us (14%)
  between operations  14.3 us (9%)
  other arithmetic  7.16 us (5%)
  local copies, waits for them, and re-layouts  6.75 us (4%)
  starting transfers between devices  3.5 us (2%)
    reduce_scatter x1, waiting for transfers between devices, local(): lax.psum_scatter((routed_partial + shared_part).astype(jnp.bfloat16), 'tp...  31.7 us
    psum x1, blocking collectives, local(): summed = lax.psum(branch.astype(jnp.bfloat16), 'tp').astype(jnp.float32)  23.9 us
    all_to_all x1, blocking collectives, local(): lax.all_to_all(picked.astype(jnp.bfloat16).reshape(n_ep, local_experts *...  13.9 us
    psum x1, blocking collectives, local(): lax.psum((jnp.sum(final_in, -1), jnp.sum(final_in * final_in, -1)), 'tp')  12.2 us
    all_gather x1, blocking collectives, local(): rows_full = lax.all_gather(hidden_in, 'tp', axis=1, tiled=True)  10.7 us
    all_to_all x1, waiting for transfers between devices, local(): lax.all_to_all(expert_part, 'ep', split_axis=0, concat_axis=0, tiled=True)  8.36 us
    dot_general x4, matrix products, project(): product = jnp.dot(rows_full, weight, preferred_element_type=jnp.float32)  7.85 us
    dot_general x1, matrix products, local(): jnp.einsum('gecf,efd->gecd', hidden_part, exp_down, preferred_element_typ...  4.99 us
  transfers between devices with their start and end apart: 2, of which 2 were waited for; matrix products, arithmetic and copies ran while one was open for 2% of the time, Pallas kernels for 0%

commit v1 on v0

--- a/solution.py
+++ b/solution.py
@@ -47,7 +47,7 @@
     expert_count = local_experts * n_ep
     capacity = max(2, 3 * seq_count * top_count // (2 * expert_count))
     slot_count = expert_count * capacity
-    rows_full = lax.all_gather(hidden_in, "tp", axis=1, tiled=True)
+    rows_full = jnp.concatenate(lax.all_gather(hidden_in, "tp"), axis=1)
 
     def project(weight):
         product = jnp.dot(rows_full, weight, preferred_element_type=jnp.float32)

time: 156 us -> 156 us (level)
  no operation moved by 1% of the time
where the time goes in v1:
time: 156 us; the launch traced here: 155 us
  blocking collectives  60.9 us (39%)
  waiting for transfers between devices  40.1 us (26%)
  matrix products  22.6 us (14%)
  between operations  14.3 us (9%)
  other arithmetic  7.16 us (5%)
  local copies, waits for them, and re-layouts  6.79 us (4%)
  starting transfers between devices  3.5 us (2%)
    reduce_scatter x1, waiting for transfers between devices, local(): lax.psum_scatter((routed_partial + shared_part).astype(jnp.bfloat16), 'tp...  31.7 us
    psum x1, blocking collectives, local(): summed = lax.psum(branch.astype(jnp.bfloat16), 'tp').astype(jnp.float32)  24 us
    all_to_all x1, blocking collectives, local(): lax.all_to_all(picked.astype(jnp.bfloat16).reshape(n_ep, local_experts *...  13.9 us
    psum x1, blocking collectives, local(): lax.psum((jnp.sum(final_in, -1), jnp.sum(final_in * final_in, -1)), 'tp')  12.1 us
    all_gather x1, blocking collectives, local(): rows_full = jnp.concatenate(lax.all_gather(hidden_in, 'tp'), axis=1)  10.9 us
    all_to_all x1, waiting for transfers between devices, local(): lax.all_to_all(expert_part, 'ep', split_axis=0, concat_axis=0, tiled=True)  8.36 us
    dot_general x4, matrix products, project(): product = jnp.dot(rows_full, weight, preferred_element_type=jnp.float32)  7.86 us
    dot_general x1, matrix products, local(): jnp.einsum('gecf,efd->gecd', hidden_part, exp_down, preferred_element_typ...  5 us
  transfers between devices with their start and end apart: 2, of which 2 were waited for; matrix products, arithmetic and copies ran while one was open for 2% of the time, Pallas kernels for 0%

profile of v1, /device:TPU:0, one launch (start us, length us, event | category | flops | bytes accessed | tf_op | source)
XLA Modules:
  0.0 155.4 jit_solution(14068929202801168686)
XLA Ops:
  7.2 0.0 copy-start
  7.2 0.9 copy.45
  8.1 0.1 eq.30
  8.2 0.1 fusion.39
  8.3 0.1 reduce_window_sum.11
  8.3 0.2 select_reduce_fusion.1
  8.5 0.1 reduce_sum.78
  8.6 0.8 copy.47
  9.4 10.9 %all-gather.1 = bf16[8,12,256]{2,1,0:T(8,128)(2,1)S(1)} all-gather(bf16[1,12,256]{2,1,0:T(8,128)(2,1)} %bitcast.106), channel_id=2, replica_groups=mesh['ep'=4,'tp'=8] {'tp'}, dimensions={0}, use_global_device_ids=true | all-gather | bytes 55296 | tf_op jit(solution)/shard_map/all_gather | solution.py:50
  20.3 2.0 %convolution_convert_fusion.2 = bf16[12,512]{1,0:T(8,128)(2,1)S(1)} fusion(bf16[12,2048]{1,0:T(8,128)(2,1)S(1)} %bitcast.85, bf16[2048,512]{1,0:T(8,128)(2,1)} %param.27), kind=kOutput, calls=%fused_computation.17 | convolution fusion | flops 25171968 | bytes 2158592 | tf_op jit(solution)/shard_map/dot_general | solution.py:53
  22.3 0.0 copy-start.2
  22.3 2.0 %convolution_convert_fusion.5 = bf16[12,512]{1,0:T(8,128)(2,1)S(1)} fusion(bf16[12,2048]{1,0:T(8,128)(2,1)S(1)} %bitcast.86, bf16[2048,512]{1,0:T(8,128)(2,1)} %param.26), kind=kOutput, calls=%fused_computation.20 | convolution fusion | flops 25171968 | bytes 2158592 | tf_op jit(solution)/shard_map/dot_general | solution.py:53
  24.4 2.0 %convolution_convert_fusion.3 = bf16[12,512]{1,0:T(8,128)(2,1)S(1)} fusion(bf16[12,2048]{1,0:T(8,128)(2,1)S(1)} %bitcast.87, bf16[2048,512]{1,0:T(8,128)(2,1)} %param.25), kind=kOutput, calls=%fused_computation.18 | convolution fusion | flops 25171968 | bytes 2158592 | tf_op jit(solution)/shard_map/dot_general | solution.py:53
  26.4 2.0 %convolution_convert_fusion.4 = bf16[12,512]{1,0:T(8,128)(2,1)S(1)} fusion(bf16[12,2048]{1,0:T(8,128)(2,1)S(1)} %bitcast.88, bf16[2048,512]{1,0:T(8,128)(2,1)} %param.24), kind=kOutput, calls=%fused_computation.19 | convolution fusion | flops 25171968 | bytes 2158592 | tf_op jit(solution)/shard_map/dot_general | solution.py:53
  28.5 3.8 %multiply_add_fusion = f32[12,4,128,128]{3,2,1,0:T(8,128)S(1)} fusion(f32[12,4,128,128]{3,2,1,0:T(8,128)} %param.22, f32[12,4,128]{2,1,0:T(4,128)S(1)} %reshape.148, f32[12,4,128]{2,1,0:T(4,128)S(1)} %bitcast.99, f32[12,4,128]{2,1,0:T(4,128)S(1)} %bitcast.98), kind=kLoop, calls=%fused_computation.6 | loop fusion | flops 2359296 | bytes 6365184 | tf_op jit(solution)/shard_map/add | solution.py:62
  32.3 0.0 copy-start.1
  32.3 1.6 %copy-done.1 = f32[12,4,128,128]{3,2,1,0:T(8,128)} copy-done((f32[12,4,128,128]{3,2,1,0:T(8,128)}, f32[12,4,128,128]{3,2,1,0:T(8,128)S(1)}, u32[]{:S(2)}) %copy-start.1) | copy-done | bytes 3145752
  34.0 2.8 %fusion.51 = f32[12,4,1,128]{3,2,1,0:T(1,128)S(1)} fusion(f32[12,4,128,1]{2,3,1,0:T(1,128)S(1)} %bitcast.97, f32[12,4,128,128]{3,2,1,0:T(8,128)S(1)} %multiply_add_fusion), kind=kOutput, calls=%fused_computation.69 | convolution fusion | flops 9437184 | bytes 3194880 | tf_op jit(solution)/shard_map/bhd,bhdv->bhv/dot_general | solution.py:63
  36.7 0.1 multiply_reduce_fusion.1
  36.8 0.1 fusion.40
  37.0 0.4 convolution_convert_fusion.1
  37.3 24.0 %psum.21 = bf16[12,2048]{1,0:T(8,128)(2,1)S(1)} all-reduce(bf16[12,2048]{1,0:T(8,128)(2,1)S(1)} %convolution_convert_fusion.1), channel_id=1, replica_groups=mesh['ep'=4,'tp'=8] {'tp'}, use_global_device_ids=true, to_apply=%region_1.2 | all-reduce | flops 24576 | bytes 98304 | tf_op jit(solution)/shard_map/psum | solution.py:67
  61.4 0.1 fusion.28
  61.5 0.2 multiply_reduce_fusion
  61.7 0.1 convert_reduce_fusion
  61.9 0.1 add_convert_fusion
  62.0 0.3 convolution_convert_fusion
  62.2 0.1 reshape.143
  62.3 13.9 %all_to_all.10 = bf16[4,18,2048]{2,1,0:T(8,128)(2,1)S(1)} all-to-all(bf16[4,18,2048]{2,1,0:T(8,128)(2,1)S(1)} %reshape.143), channel_id=1, replica_groups=mesh['ep'=4,'tp'=8] {'ep'}, dimensions={0} | all-to-all | bytes 589824 | tf_op jit(solution)/shard_map/all_to_all | solution.py:90
  76.2 0.2 copy.48
  76.4 2.9 %fusion.13 = f32[4,2,9,512]{3,2,0,1:T(8,128)S(1)} fusion(bf16[2,2048,512]{2,1,0:T(8,128)(2,1)} %param.34, bf16[4,2,9,2048]{3,0,2,1:T(4,128)(2,1)S(1)} %bitcast.83), kind=kOutput, calls=%fused_computation.13 | convolution fusion | flops 150994944 | bytes 4636672 | tf_op jit(solution)/shard_map/gecd,edf->gecf/dot_general | solution.py:98
  79.4 5.0 %fusion.9 = bf16[4,2,9,2048]{3,2,0,1:T(8,128)(2,1)S(1)} fusion(bf16[2,512,2048]{2,1,0:T(8,128)(2,1)} %param.36, bf16[2,2048,512]{2,1,0:T(8,128)(2,1)} %param.35, bf16[4,2,9,2048]{3,0,2,1:T(4,128)(2,1)S(1)} %bitcast.84, f32[4,2,9,512]{3,2,0,1:T(8,128)S(1)} %fusion.13), kind=kOutput, calls=%fused_computation.8 | convolution fusion | flops 302358528 | bytes 9125888 | tf_op jit(solution)/shard_map/gecf,efd->gecd/dot_general | solution.py:101
  84.4 0.3 copy.51
  84.6 0.9 copy.52
  85.5 3.5 %all-to-all-start.1 = ((bf16[4,18,2048]{2,1,0:T(8,128)(2,1)}), bf16[4,18,2048]{2,1,0:T(8,128)(2,1)S(1)}, u32[]{:S(2)}, u32[]{:S(2)}) async-start(bf16[4,18,2048]{2,1,0:T(8,128)(2,1)} %copy.52), calls=%async_computation.1 | async-start | bytes 786432 | tf_op jit(solution)/shard_map/all_to_all | solution.py:112
  89.0 0.0 reduce-scatter.2.cloned.1.call-start
  89.1 1.1 fusion.53
  90.2 8.4 %all-to-all-done.1 = bf16[4,18,2048]{2,1,0:T(8,128)(2,1)S(1)} async-done(((bf16[4,18,2048]{2,1,0:T(8,128)(2,1)}), bf16[4,18,2048]{2,1,0:T(8,128)(2,1)S(1)}, u32[]{:S(2)}, u32[]{:S(2)}) %all-to-all-start.1) | async-done | bytes 294944 | tf_op jit(solution)/shard_map/all_to_all | solution.py:112
  98.5 0.1 reshape.145
  98.6 0.2 fusion.52
  98.9 2.0 %fusion.12 = bf16[12,2048]{1,0:T(8,128)(2,1)} fusion(f32[12,2048]{1,0:T(8,128)S(1)} %fusion.52, bf16[64,2048]{1,0:T(8,128)(2,1)} %param.39, bf16[12,2048]{1,0:T(8,128)(2,1)S(1)} %add_convert_fusion, bf16[2048,64]{0,1:T(8,128)(2,1)} %param.38, f32[12,64]{1,0:T(8,128)S(1)} %fusion.53), kind=kOutput, calls=%fused_computation.11 | convolution fusion | flops 6345216 | bytes 723968 | tf_op jit(solution)/shard_map/dot_general | solution.py:111
  100.9 0.0 reduce-scatter.2.cloned.1.call-update
  101.0 0.8 dynamic_slice.11
  101.7 0.8 dynamic_slice.10
  102.5 31.7 %reduce-scatter.2.cloned.1.call-done = bf16[12,256]{1,0:T(8,128)(2,1)} async-done(((bf16[12,2048]{1,0:T(8,128)(2,1)}), bf16[12,256]{1,0:T(8,128)(2,1)}) %reduce-scatter.2.cloned.1.call-update) | async-done | bytes 6160 | tf_op jit(solution)/shard_map/reduce_scatter | solution.py:118
  134.2 0.8 fusion.41
  135.0 12.1 %all-reduce = (f32[12]{0:T(128)S(1)}, f32[12]{0:T(128)S(1)}) all-reduce(f32[12]{0:T(128)S(1)} %get-tuple-element.3, f32[12]{0:T(128)S(1)} %get-tuple-element.2), channel_id=1, replica_groups=mesh['ep'=4,'tp'=8] {'tp'}, use_global_device_ids=true, to_apply=%region_12.13 | all-reduce | flops 24 | bytes 192 | tf_op jit(solution)/shard_map/psum | solution.py:122
  147.2 1.4 add_convert_fusion.1
  (29 shorter events, 0.3 us)
Async XLA Ops:
  7.2 29.8 %copy-start = (bf16[512,2048]{1,0:T(8,128)(2,1)S(1)}, bf16[512,2048]{1,0:T(8,128)(2,1)}, u32[]{:S(2)}) copy-start(bf16[512,2048]{1,0:T(8,128)(2,1)} %param.29) | copy-start | bytes 6291460
  22.3 6.1 %copy-start.2 = (f32[4,128]{1,0:T(4,128)S(1)}, f32[4,128]{1,0:T(4,128)}, u32[]{:S(2)}) copy-start(f32[4,128]{1,0:T(4,128)} %param.23) | copy-start | bytes 6148
  32.3 1.7 %copy-start.1 = (f32[12,4,128,128]{3,2,1,0:T(8,128)}, f32[12,4,128,128]{3,2,1,0:T(8,128)S(1)}, u32[]{:S(2)}) copy-start(f32[12,4,128,128]{3,2,1,0:T(8,128)S(1)} %multiply_add_fusion) | copy-start | bytes 9437188
  32.3 4.5 %copy-start.5 = (f32[128]{0:T(128)S(1)}, f32[128]{0:T(128)}, u32[]{:S(2)}) copy-start(f32[128]{0:T(128)} %param.28) | copy-start | bytes 1540
  32.3 29.6 %copy-start.3 = (f32[2048]{0:T(1024)S(1)}, f32[2048]{0:T(1024)}, u32[]{:S(2)}) copy-start(f32[2048]{0:T(1024)} %param.31) | copy-start | bytes 24580
  32.3 29.6 %copy-start.4 = (f32[2048]{0:T(1024)S(1)}, f32[2048]{0:T(1024)}, u32[]{:S(2)}) copy-start(f32[2048]{0:T(1024)} %param.30) | copy-start | bytes 24580
  85.5 13.0 %all-to-all-start.1 = ((bf16[4,18,2048]{2,1,0:T(8,128)(2,1)}), bf16[4,18,2048]{2,1,0:T(8,128)(2,1)S(1)}, u32[]{:S(2)}, u32[]{:S(2)}) async-start(bf16[4,18,2048]{2,1,0:T(8,128)(2,1)} %copy.52), calls=%async_computation.1 | async-start | bytes 786432 | tf_op jit(solution)/shard_map/all_to_all | solution.py:112
  89.0 45.2 %reduce-scatter.2.cloned.1.call-start = ((), (), s32[]{:S(2)}) async-start(), calls=%async_computation.3 | async-start | bytes 73728 | tf_op jit(solution)/shard_map/reduce_scatter | solution.py:118
Sparse Core Ops, SparseCore 0:
  101.1 33.0 reduce-scatter.1
